TPU v7x, 32 devices: a whole 2x2x4 slice. The times are simulated.
32 devices in a mesh: sp: 16 (over z, y, core), tp: 2 (over x).
Axes of the slice: x: 2, y: 2, z: 4, core: 2. Of those that a mesh axis runs over, the one named last changes fastest.
Arguments:
- layer_source_rows: bfloat16 [6144, 2048], P(('sp', 'tp')), may hold values from -6 to 6
- entry_rescale_factor: bfloat16 [2048], replicated, may hold values from 0.099609375 to 1.8984375
- sliding_mixer_entry_matrix: bfloat16 [3, 2048, 1024], P(None, 'sp', 'tp'), may hold values from -0.125 to 0.125
- recurrent_mixer_entry_matrix: bfloat16 [2, 2048, 1024], P(None, 'sp', 'tp'), may hold values from -0.125 to 0.125
- latent_write_read_matrix: bfloat16 [2, 2048, 2048], P(None, 'sp', 'tp'), may hold values from -0.125 to 0.125
- timestep_matrix: bfloat16 [2048, 2, 16], P(None, None, 'tp'), may hold values from -0.125 to 0.125
- sliding_kernel_coefficients: bfloat16 [3, 1024], P(None, 'tp'), may hold values from -3.5 to 3.5
- recurrent_kernel_coefficients: bfloat16 [5, 1024], P(None, 'tp'), may hold values from -0.5 to 0.5
- latent_kernel_coefficients: bfloat16 [5, 2, 2048], P(None, None, 'tp'), may hold values from -0.5 to 0.5
- lane_forgetting_rate: float32 [2, 16], P(None, 'tp'), may hold values from 0 to 1
- spike_forgetting_rate: float32 [6144, 16], P('sp', 'tp'), may hold values from -2 to 0
- lane_rescale_factor: bfloat16 [1024], P('tp'), may hold values from 0.099609375 to 1.8984375
- sliding_mixer_exit_matrix: bfloat16 [1024, 2048], P('tp', 'sp'), may hold values from -0.125 to 0.125
- recurrent_mixer_exit_matrix: bfloat16 [1024, 2048], P('tp', 'sp'), may hold values from -0.125 to 0.125
Outputs:
- mixed_out: bfloat16 [6144, 2048], P(('sp', 'tp'))
All inputs are finite; a program needn't handle non-finite values.
Results may differ from a plain program's by a relative error of at most 0.017.
Values may be sent and summed in bfloat16 or wider, within the bound.
No kernel may reach another device: no remote copies, remote signals or barrier semaphores. Data moves between devices by JAX's collectives and lax.ppermute only.
A program may use at most 64 MiB of HBM per device.

v0:
```python
import jax
import jax.numpy as jnp
from jax import lax
from jax.sharding import PartitionSpec as P

HEAD_DIM = 64
STATE = 128
BLOCK = 128
HALO = 8
epsilon = 1e-05


def swapped(value, axis, distance):
    size = lax.axis_size(axis)
    return lax.ppermute(value, axis, [(i, i ^ distance) for i in range(size)])


def tp_rows(normed):
    if lax.axis_size("tp") != 2:
        return lax.all_gather(normed, "tp", axis=0, tiled=True)
    mine = lax.axis_index("tp")
    count = normed.shape[0]
    other = swapped(normed, "tp", 1)
    rows = jnp.zeros((2 * count, normed.shape[1]), normed.dtype)
    rows = lax.dynamic_update_slice(rows, normed, (mine * count, 0))
    return lax.dynamic_update_slice(rows, other, ((1 - mine) * count, 0))


def with_halo(rows):
    size = lax.axis_size("sp")
    up = [(i, i + 1) for i in range(size - 1)]
    down = [(i + 1, i) for i in range(size - 1)]
    before = lax.ppermute(rows[-HALO:], "sp", up)
    after = lax.ppermute(rows[:HALO], "sp", down)
    return jnp.concatenate([before, rows, after], axis=0)


def apply_taps(padded, tap_table, length):
    taps = tap_table.shape[0]
    first = HALO - taps // 2
    summed = jnp.zeros((length, padded.shape[1]), jnp.float32)
    for offset in range(taps):
        summed = summed + padded[first + offset : first + offset + length].astype(
            jnp.float32
        ) * tap_table[offset].astype(jnp.float32)
    return summed


def decay_levels(decay):
    place = lax.axis_index("sp")
    levels = []
    ahead = jnp.ones_like(decay)
    distance = 1
    while distance < lax.axis_size("sp"):
        other = swapped(decay, "sp", distance)
        upper = place & distance != 0
        joins = jnp.stack([upper, ~upper])
        levels.append((distance, joins[:, None], decay, other, ahead))
        ahead = jnp.where(joins[:, None], ahead * other, ahead)
        decay = decay * other
        distance *= 2
    return levels


def entering_state(total, levels):
    place = lax.axis_index("sp")
    prefix = jnp.zeros_like(total)
    for number, (distance, joins, own, other, ahead) in enumerate(levels):
        wide = lambda a: a[..., None, None]
        joins = joins[None, :, :, None]
        if number + 1 < len(levels):
            got = swapped(total.astype(jnp.bfloat16), "sp", distance).astype(jnp.float32)
            prefix = jnp.where(joins, got * wide(ahead) + prefix, prefix)
            total = jnp.where(joins, got * wide(own) + total, total * wide(other) + got)
        else:
            upper = place & distance != 0
            send = jnp.where(upper, total[:, 1], total[:, 0]).astype(jnp.bfloat16)
            got = swapped(send, "sp", distance).astype(jnp.float32)
            prefix = jnp.where(joins, got[:, None] * wide(ahead) + prefix, prefix)
    return prefix


def local(
    layer_source_rows,
    entry_rescale_factor,
    sliding_mixer_entry_matrix,
    recurrent_mixer_entry_matrix,
    latent_write_read_matrix,
    timestep_matrix,
    sliding_kernel_coefficients,
    recurrent_kernel_coefficients,
    latent_kernel_coefficients,
    lane_forgetting_rate,
    spike_forgetting_rate,
    lane_rescale_factor,
    sliding_mixer_exit_matrix,
    recurrent_mixer_exit_matrix,
):
    f32, bf16 = (jnp.float32, jnp.bfloat16)
    conv_width = sliding_mixer_entry_matrix.shape[2]
    ssd_width = recurrent_mixer_entry_matrix.shape[2]
    state_width = latent_write_read_matrix.shape[2]
    heads = timestep_matrix.shape[2]
    assert state_width == heads * STATE and ssd_width == heads * HEAD_DIM
    ssd_shard = jnp.concatenate(
        [
            recurrent_mixer_entry_matrix[0],
            recurrent_mixer_entry_matrix[1],
            latent_write_read_matrix[0],
            latent_write_read_matrix[1],
        ],
        axis=1,
    )
    ssd_weight = lax.all_gather(ssd_shard, "sp", axis=0, tiled=True)
    float_rows = layer_source_rows.astype(f32)
    normed = (
        float_rows
        * lax.rsqrt(jnp.mean(float_rows * float_rows, axis=-1, keepdims=True) + epsilon)
        * entry_rescale_factor.astype(f32)
    ).astype(bf16)
    rows = tp_rows(normed)
    length = rows.shape[0]
    exit_shard = jnp.concatenate([sliding_mixer_exit_matrix, recurrent_mixer_exit_matrix], axis=0).T
    conv_shard = jnp.concatenate(
        [sliding_mixer_entry_matrix[k] for k in range(3)] + [exit_shard], axis=1
    )
    conv_shard, rows = lax.optimization_barrier((conv_shard, rows))
    conv_weight = lax.all_gather(conv_shard, "sp", axis=0, tiled=True)
    wide_rows = with_halo(rows)
    raw_step = (
        jnp.dot(rows, timestep_matrix.reshape(-1, 2 * heads), preferred_element_type=f32)
        .astype(bf16)
        .astype(f32)
        .reshape(length, 2, heads)
    )
    deltas = jax.nn.softplus(raw_step)
    log_decay = -deltas * lane_forgetting_rate[None] + spike_forgetting_rate[:, None, :]
    blocks = length // BLOCK
    order = jnp.arange(BLOCK)
    lower = (order[:, None] >= order[None, :]).astype(f32)
    sums = jnp.stack([lower, lower.T])
    logs = log_decay.reshape(blocks, BLOCK, 2, heads).transpose(2, 3, 0, 1)
    delta = deltas.reshape(blocks, BLOCK, 2, heads).transpose(2, 3, 0, 1)
    running = jnp.einsum("dhbs,dts->dhbt", logs, sums, precision=lax.Precision.HIGHEST)
    ends = jnp.stack([running[0, :, :, -1], running[1, :, :, 0]])
    to_end = jnp.exp(ends[..., None] - running) * delta
    levels = decay_levels(jnp.exp(jnp.sum(ends, axis=-1)))
    levels = [(n, j, a.T, b.T, c.T) for n, j, a, b, c in levels]
    before_ends = jnp.cumsum(ends[0], axis=-1) - ends[0]
    after_ends = jnp.cumsum(ends[1][:, ::-1], axis=-1)[:, ::-1] - ends[1]
    starts = jnp.exp(jnp.stack([before_ends, after_ends]))
    mask = order[:, None] >= order[None, :]
    gaps = running[..., :, None] - running[..., None, :]
    decays = (
        jnp.where(mask, jnp.exp(jnp.where(mask, gaps[0], 0.0)), 0.0) * delta[0][..., None, :]
        + jnp.where(mask.T, jnp.exp(jnp.where(mask.T, gaps[1], 0.0)), 0.0) * delta[1][..., None, :]
    )
    projected = jnp.dot(wide_rows, ssd_weight, preferred_element_type=f32).astype(bf16)
    ssd_gate = projected[HALO : HALO + length, :ssd_width]
    joined_taps = jnp.concatenate(
        [
            recurrent_kernel_coefficients,
            latent_kernel_coefficients.reshape(latent_kernel_coefficients.shape[0], -1),
        ],
        axis=1,
    )
    mixed = jax.nn.silu(apply_taps(projected[:, ssd_width:], joined_taps, length)).astype(bf16)
    ssd_x = mixed[:, :ssd_width].reshape(blocks, BLOCK, heads, HEAD_DIM)
    keys_b = mixed[:, ssd_width : ssd_width + state_width].reshape(blocks, BLOCK, heads, STATE)
    reads_c = mixed[:, ssd_width + state_width :].reshape(blocks, BLOCK, heads, STATE)
    ssd_x = ssd_x.transpose(2, 0, 1, 3)
    keys_b = keys_b.transpose(2, 0, 1, 3)
    reads_c = reads_c.transpose(2, 0, 1, 3)
    x_float = ssd_x.astype(f32)
    weighted = jnp.concatenate(
        [(x_float * to_end[d][..., None]).astype(bf16) for d in range(2)], axis=-1
    )
    contribution = jnp.einsum("hbsp,hbsn->hbpn", weighted, keys_b, preferred_element_type=f32)
    contribution = contribution.reshape(heads, blocks, 2, HEAD_DIM, STATE)
    end_decay = jnp.exp(ends)[..., None, None]
    forward, fore = ([], jnp.zeros((heads, HEAD_DIM, STATE), f32))
    for b in range(blocks):
        forward.append(fore)
        fore = fore * end_decay[0, :, b] + contribution[:, b, 0]
    backward, aft = ([None] * blocks, jnp.zeros((heads, HEAD_DIM, STATE), f32))
    for b in reversed(range(blocks)):
        backward[b] = aft
        aft = aft * end_decay[1, :, b] + contribution[:, b, 1]
    prefix = entering_state(jnp.stack([fore, aft], axis=1), levels)
    scores = jnp.einsum("hbtn,hbsn->hbts", reads_c, keys_b, preferred_element_type=f32)
    within = jnp.einsum(
        "hbts,hbsp->hbtp", (scores * decays).astype(bf16), ssd_x, preferred_element_type=f32
    )
    inside = jnp.stack([jnp.stack(forward, 1), jnp.stack(backward, 1)], axis=2)
    entering = inside + prefix[:, None] * starts.transpose(1, 2, 0)[..., None, None]
    entering = entering.astype(bf16).reshape(heads, blocks, 2 * HEAD_DIM, STATE)
    carried = jnp.einsum("hbtn,hbpn->hbtp", reads_c, entering, preferred_element_type=f32)
    grown = jnp.exp(running)[..., None]
    y = within + carried[..., :HEAD_DIM] * grown[0] + carried[..., HEAD_DIM:] * grown[1]
    gate = ssd_gate.astype(f32).reshape(blocks, BLOCK, heads, HEAD_DIM).transpose(2, 0, 1, 3)
    y = y * jax.nn.silu(gate)
    y = y * lax.rsqrt(jnp.mean(y * y, axis=-1, keepdims=True) + epsilon)
    y = y * lane_rescale_factor.astype(f32).reshape(heads, 1, 1, HEAD_DIM)
    y_ssd = y.astype(bf16).transpose(1, 2, 0, 3).reshape(length, ssd_width)
    conv = jnp.dot(wide_rows, conv_weight[:, : 3 * conv_width], preferred_element_type=f32).astype(
        bf16
    )
    out_gate = conv[HALO : HALO + length, :conv_width].astype(f32)
    gated_in = (
        conv[:, conv_width : 2 * conv_width].astype(f32) * conv[:, 2 * conv_width :].astype(f32)
    ).astype(bf16)
    y_conv = (out_gate * apply_taps(gated_in, sliding_kernel_coefficients, length)).astype(bf16)
    mixed_y = jnp.concatenate([y_conv, y_ssd], axis=1)
    exit_weight = conv_weight[:, 3 * conv_width :]

    def leave(part):
        return lax.dot_general(
            part, exit_weight, (((1,), (1,)), ((), ())), preferred_element_type=f32
        ).astype(bf16)

    if lax.axis_size("tp") != 2:
        return lax.psum_scatter(leave(mixed_y), "tp", scatter_dimension=0, tiled=True)
    mine = lax.axis_index("tp")
    half = length // 2
    sent = leave(lax.dynamic_slice_in_dim(mixed_y, (1 - mine) * half, half, 0))
    got = swapped(sent, "tp", 1)
    kept = leave(lax.dynamic_slice_in_dim(mixed_y, mine * half, half, 0))
    return (kept.astype(f32) + got.astype(f32)).astype(bf16)


def solution(mesh):
    placed = (
        P(("sp", "tp"), None),
        P(),
        P(None, "sp", "tp"),
        P(None, "sp", "tp"),
        P(None, "sp", "tp"),
        P(None, None, "tp"),
        P(None, "tp"),
        P(None, "tp"),
        P(None, None, "tp"),
        P(None, "tp"),
        P("sp", "tp"),
        P("tp"),
        P("tp", "sp"),
        P("tp", "sp"),
    )
    return jax.shard_map(
        local, mesh=mesh, in_specs=placed, out_specs=P(("sp", "tp"), None), check_vma=False
    )
```

profile of v0, /device:TPU:0, one launch (start us, length us, event | category | flops | bytes accessed | tf_op | source)
XLA Modules:
  0.0 282.8 jit_solution(1260736302038786378)
XLA Ops:
  6.5 1.1 slice_bitcast_fusion.11
  7.7 1.1 slice_bitcast_fusion.13
  8.7 0.9 pad_maximum_fusion.1
  10.5 3.0 %collective-permute-start = (bf16[192,2048]{1,0:T(8,128)(2,1)S(1)}, bf16[192,2048]{1,0:T(8,128)(2,1)S(1)}, u32[]{:S(2)}, u32[]{:S(2)}) collective-permute-start(bf16[192,2048]{1,0:T(8,128)(2,1)S(1)} %get-tuple-element.25), channel_id=1, source_target_pairs={{0,1},{1,0},{2,3},{3,2},{4,5},{5,4},{6,7},{7,6},{8,9},{9,8},{10,11... | collective-permute-start | bytes 2359304 | tf_op jit(solution)/shard_map/ppermute | solution.py:15
  13.5 1.8 fusion.125
  15.4 1.0 copy.146
  16.4 1.7 copy.147
  18.1 1.0 maximum_bitcast_fusion.2
  19.1 1.8 pad_maximum_fusion.2
  21.0 10.1 %collective-permute-done = bf16[192,2048]{1,0:T(8,128)(2,1)S(1)} collective-permute-done((bf16[192,2048]{1,0:T(8,128)(2,1)S(1)}, bf16[192,2048]{1,0:T(8,128)(2,1)S(1)}, u32[]{:S(2)}, u32[]{:S(2)}) %collective-permute-start) | collective-permute-done | bytes 786464 | tf_op jit(solution)/shard_map/ppermute | solution.py:15
  31.2 0.7 reshape.309
  32.7 0.6 iota_compare_fusion
  35.4 2.4 collective-permute-start.1
  37.8 1.3 collective-permute-start.2
  39.5 0.6 copy.132
  40.1 0.6 copy.133
  40.7 0.6 copy.106
  41.4 0.6 fusion.110
  42.0 2.2 broadcast_subtract_fusion
  44.1 0.6 copy.107
  44.7 3.6 %collective-permute-start.6 = (f32[2,8]{1,0:T(2,128)S(1)}, f32[2,8]{1,0:T(2,128)S(1)}, u32[]{:S(2)}, u32[]{:S(2)}) collective-permute-start(f32[2,8]{1,0:T(2,128)S(1)} %get-tuple-element.64), channel_id=1, source_target_pairs={{0,4},{2,6},{4,0},{6,2},{8,12},{10,14},{12,8},{14,10},{16,20},{18,... | collective-permute-start | bytes 200 | tf_op jit(solution)/shard_map/ppermute | solution.py:15
  48.6 1.3 collective-permute-done.6
  49.9 3.0 %collective-permute-start.8 = (f32[2,8]{1,0:T(2,128)S(1)}, f32[2,8]{1,0:T(2,128)S(1)}, u32[]{:S(2)}, u32[]{:S(2)}) collective-permute-start(f32[2,8]{1,0:T(2,128)S(1)} %mul.523), channel_id=1, source_target_pairs={{0,8},{2,10},{4,12},{6,14},{8,0},{10,2},{12,4},{14,6},{16,24},{18,... | collective-permute-start | bytes 200 | tf_op jit(solution)/shard_map/ppermute | solution.py:15
  52.9 0.7 copy.124
  53.7 0.8 collective-permute-done.8
  54.6 0.7 copy.125
  55.2 0.7 copy.126
  55.9 0.7 copy.127
  56.6 0.7 copy.128
  57.2 0.6 constant_dynamic-update-slice_fusion.2
  57.8 1.2 constant_dynamic-update-slice_fusion.1
  59.1 0.6 constant_dynamic-update-slice_fusion
  59.7 53.7 %all-gather.5.cloned.1.call-done = bf16[2048,3072]{1,0:T(8,128)(2,1)} async-done(((bf16[128,3072]{1,0:T(8,128)(2,1)}), bf16[2048,3072]{1,0:T(8,128)(2,1)}) %all-gather.5.cloned.1.call-update) | async-done | bytes 12582928 | tf_op jit(solution)/shard_map/all_gather | solution.py:114
  113.4 8.7 %convolution_convert_fusion = bf16[400,3072]{1,0:T(8,128)(2,1)S(1)} fusion(bf16[400,2048]{1,0:T(8,128)(2,1)} %constant_dynamic-update-slice_fusion, bf16[2048,3072]{1,0:T(8,128)(2,1)} %all-gather.5.cloned.1.call-done), kind=kOutput, calls=%fused_computation.2 | convolution fusion | flops 5034393600 | bytes 16678912 | tf_op jit(solution)/shard_map/dot_general | solution.py:158
  122.1 4.2 %multiply_convert_fusion = bf16[384,2560]{1,0:T(8,128)(2,1)} fusion(bf16[400,3072]{1,0:T(8,128)(2,1)S(1)} %convolution_convert_fusion, f32[2560]{0:T(1024)S(1)} %get-tuple-element.10, f32[2560]{0:T(1024)S(1)} %get-tuple-element.11, f32[2560]{0:T(1024)S(1)} %get-tuple-element.12, f32[2560]{0:T(1024)S(1)} %get-tuple-element.13, f32[2560]{0:T(1024)S(1)} %get-tuple-element.9), kind=kLoop, calls=%fused_computation.3 | loop fusion | flops 18677760 | bytes 11847680 | tf_op jit(solution)/shard_map/convert_element_type | solution.py:167
  126.3 1.8 slice.271
  128.0 1.7 reshape.312
  129.7 1.2 copy.109
  131.0 2.4 slice_bitcast_fusion.3
  134.5 1.1 fusion.83
  136.0 68.2 %all-gather.3.cloned.1.call-done = bf16[2048,2560]{0,1:T(8,128)(2,1)} async-done(((bf16[128,2560]{0,1:T(8,128)(2,1)}), bf16[2048,2560]{0,1:T(8,128)(2,1)}) %all-gather.3.cloned.1.call-update) | async-done | bytes 10485776 | tf_op jit(solution)/shard_map/all_gather | solution.py:128
  204.2 6.0 %fusion.6 = bf16[400,1536]{1,0:T(8,128)(2,1)S(1)} fusion(bf16[400,2048]{1,0:T(8,128)(2,1)} %constant_dynamic-update-slice_fusion, bf16[2048,2560]{0,1:T(8,128)(2,1)} %all-gather.3.cloned.1.call-done), kind=kOutput, calls=%fused_computation.8 | convolution fusion | flops 2517196800 | bytes 9158656 | tf_op jit(solution)/shard_map/dot_general | solution.py:205
  210.6 1.5 collective-permute-start.5
  212.2 1.1 multiply_convert_fusion.3
  213.3 5.8 %collective-permute-done.5 = bf16[8,2,64,128]{3,2,1,0:T(8,128)(2,1)S(1)} collective-permute-done((bf16[8,2,64,128]{3,2,1,0:T(8,128)(2,1)S(1)}, bf16[8,2,64,128]{3,2,1,0:T(8,128)(2,1)S(1)}, u32[]{:S(2)}, u32[]{:S(2)}) %collective-permute-start.5) | collective-permute-done | bytes 262176 | tf_op jit(solution)/shard_map/ppermute | solution.py:15
  219.1 1.1 fusion.90
  220.2 1.0 slice_convert_fusion
  221.2 1.1 copy.155
  222.7 1.4 copy.135
  224.2 1.1 maximum_bitcast_fusion
  225.4 2.8 collective-permute-done.7
  228.2 1.4 fusion.69
  229.6 1.6 collective-permute-start.9
  231.4 6.0 %collective-permute-done.9 = bf16[8,64,128]{2,1,0:T(8,128)(2,1)S(1)} collective-permute-done((bf16[8,64,128]{2,1,0:T(8,128)(2,1)S(1)}, bf16[8,64,128]{2,1,0:T(8,128)(2,1)S(1)}, u32[]{:S(2)}, u32[]{:S(2)}) %collective-permute-start.9) | collective-permute-done | bytes 131104 | tf_op jit(solution)/shard_map/ppermute | solution.py:15
  237.4 1.3 add_select_fusion
  239.2 0.6 copy-done.5
  239.8 1.8 fusion.49
  241.7 5.2 %multiply_reduce_fusion = (f32[8,3,128]{2,1,0:T(4,128)}, f32[8,3,128,64]{2,3,1,0:T(8,128)}) fusion(f32[3,128,8,64]{1,3,0,2:T(8,128)} %copy.135, f32[8,3,128]{2,1,0:T(4,128)} %copy.133, f32[8,3,128,128]{2,3,1,0:T(8,128)} %fusion.49, f32[8,3,128]{2,1,0:T(4,128)} %copy.132, bf16[3,128,8,64]{1,3,0,2:T(8,128)(2,1)S(1)} %copy-done.9, ...), kind=kOutput, calls=%fused_computation.73 | convolution fusion | flops 156693504 | bytes 8351744 | tf_op jit(solution)/shard_map/hbts,hbsp->hbtp/dot_general | solution.py:191
  246.8 0.7 add_rsqrt_fusion
  247.6 1.4 fusion.71
  249.9 3.2 %fusion.15 = bf16[192,2048]{1,0:T(8,128)(2,1)S(1)} fusion(bf16[2048,2560]{0,1:T(8,128)(2,1)} %all-gather.3.cloned.1.call-done, s32[]{:T(128)S(6)} %select_n.69, bf16[384,512]{1,0:T(8,128)(2,1)S(1)} %copy-done.13, bf16[384,512]{1,0:T(8,128)(2,1)S(1)} %reshape.314), kind=kOutput, calls=%fused_computation.11 | convolution fusion | flops 806486016 | bytes 5767172 | tf_op jit(solution)/shard_map/dot_general | solution.py:217
  253.1 1.5 collective-permute-start.10
  254.6 17.2 %collective-permute-done.10 = bf16[192,2048]{1,0:T(8,128)(2,1)S(1)} collective-permute-done((bf16[192,2048]{1,0:T(8,128)(2,1)S(1)}, bf16[192,2048]{1,0:T(8,128)(2,1)S(1)}, u32[]{:S(2)}, u32[]{:S(2)}) %collective-permute-start.10) | collective-permute-done | bytes 786464 | tf_op jit(solution)/shard_map/ppermute | solution.py:15
  271.8 4.1 %add_convert_fusion = bf16[192,2048]{1,0:T(8,128)(2,1)} fusion(bf16[192,2048]{1,0:T(8,128)(2,1)S(1)} %collective-permute-done.10, bf16[2048,2560]{0,1:T(8,128)(2,1)} %all-gather.3.cloned.1.call-done, s32[]{:T(128)S(6)} %select_n.68, bf16[384,512]{1,0:T(8,128)(2,1)S(1)} %copy-done.13, bf16[384,512]{1,0:T(8,128)(2,1)S(1)} %reshape.314), kind=kOutput, calls=%fused_computation.33 | convolution fusion | flops 808058880 | bytes 6553604 | tf_op jit(solution)/shard_map/dot_general | solution.py:217
  (156 shorter events, 8.5 us)
Async XLA Ops:
  6.5 27.6 %copy-start = (bf16[2048,2,8]{0,2,1:T(8,128)(2,1)S(1)}, bf16[2048,2,8]{0,2,1:T(8,128)(2,1)}, u32[]{:S(2)}) copy-start(bf16[2048,2,8]{0,2,1:T(8,128)(2,1)} %param.19) | copy-start | bytes 196612
  6.5 106.9 %all-gather.5.cloned.1.call-start = ((), (), s32[]{:S(2)}) async-start(), calls=%async_computation.1 | async-start | bytes 13369344 | tf_op jit(solution)/shard_map/all_gather | solution.py:114
  7.6 2.1 copy-start.32
  7.7 2.1 copy-start.3
  9.7 194.5 %all-gather.3.cloned.1.call-start = ((), (), s32[]{:S(2)}) async-start(), calls=%async_computation | async-start | bytes 11141120 | tf_op jit(solution)/shard_map/all_gather | solution.py:128
  10.5 20.6 %collective-permute-start = (bf16[192,2048]{1,0:T(8,128)(2,1)S(1)}, bf16[192,2048]{1,0:T(8,128)(2,1)S(1)}, u32[]{:S(2)}, u32[]{:S(2)}) collective-permute-start(bf16[192,2048]{1,0:T(8,128)(2,1)S(1)} %get-tuple-element.25), channel_id=1, source_target_pairs={{0,1},{1,0},{2,3},{3,2},{4,5},{5,4},{6,7},{7,6},{8,9},{9,8},{10,11... | collective-permute-start | bytes 2359304 | tf_op jit(solution)/shard_map/ppermute | solution.py:15
  19.1 12.1 %copy-start.14 = (bf16[5,2,1024]{2,1,0:T(2,128)(2,1)S(1)}, bf16[5,2,1024]{2,1,0:T(2,128)(2,1)}, u32[]{:S(2)}) copy-start(bf16[5,2,1024]{2,1,0:T(2,128)(2,1)} %param.22) | copy-start | bytes 61444
  19.1 12.1 %copy-start.35 = (bf16[512]{0:T(512)(128)(2,1)S(1)}, bf16[512]{0:T(512)(128)(2,1)}, u32[]{:S(2)}) copy-start(bf16[512]{0:T(512)(128)(2,1)} %param.25) | copy-start | bytes 3076
  19.1 13.6 %copy-start.29 = (bf16[5,512]{1,0:T(8,128)(2,1)S(1)}, bf16[5,512]{1,0:T(8,128)(2,1)}, u32[]{:S(2)}) copy-start(bf16[5,512]{1,0:T(8,128)(2,1)} %param.21) | copy-start | bytes 15364
  19.1 14.4 %copy-start.23 = (bf16[3,512]{1,0:T(4,128)(2,1)S(1)}, bf16[3,512]{1,0:T(4,128)(2,1)}, u32[]{:S(2)}) copy-start(bf16[3,512]{1,0:T(4,128)(2,1)} %param.20) | copy-start | bytes 9220
  31.1 3.5 %copy-start.37 = (f32[384,8]{0,1:T(8,128)S(1)}, f32[384,8]{0,1:T(8,128)}, u32[]{:S(2)}) copy-start(f32[384,8]{0,1:T(8,128)} %param.24) | copy-start | bytes 36868
  31.1 3.5 %copy-start.38 = (f32[2,8]{1,0:T(2,128)S(1)}, f32[2,8]{1,0:T(2,128)}, u32[]{:S(2)}) copy-start(f32[2,8]{1,0:T(2,128)} %param.23) | copy-start | bytes 196
  32.0 22.5 %copy-start.21 = (pred[2]{0:T(512)(128)(4,1)}, pred[2]{0:T(512)(128)(4,1)S(1)}, u32[]{:S(2)}) copy-start(pred[2]{0:T(512)(128)(4,1)S(1)} %pad_add_fusion.3) | copy-start | bytes 10
  32.1 22.4 %copy-start.24 = (pred[2]{0:T(512)(128)(4,1)}, pred[2]{0:T(512)(128)(4,1)S(1)}, u32[]{:S(2)}) copy-start(pred[2]{0:T(512)(128)(4,1)S(1)} %pad_add_fusion.2) | copy-start | bytes 10
  32.1 22.3 %copy-start.30 = (pred[2]{0:T(512)(128)(4,1)}, pred[2]{0:T(512)(128)(4,1)S(1)}, u32[]{:S(2)}) copy-start(pred[2]{0:T(512)(128)(4,1)S(1)} %pad_add_fusion.1) | copy-start | bytes 10
  35.2 9.5 %collective-permute-start.4 = (f32[2,8]{1,0:T(2,128)S(1)}, f32[2,8]{1,0:T(2,128)S(1)}, u32[]{:S(2)}, u32[]{:S(2)}) collective-permute-start(f32[2,8]{1,0:T(2,128)S(1)} %exp.52), channel_id=1, source_target_pairs={{0,2},{2,0},{4,6},{6,4},{8,10},{10,8},{12,14},{14,12},{16,18},{18,... | collective-permute-start | bytes 200 | tf_op jit(solution)/shard_map/ppermute | solution.py:15
  35.4 21.8 %collective-permute-start.1 = (bf16[8,2048]{1,0:T(8,128)(2,1)S(1)}, bf16[8,2048]{1,0:T(8,128)(2,1)S(1)}, u32[]{:S(2)}, u32[]{:S(2)}) collective-permute-start(bf16[8,2048]{1,0:T(8,128)(2,1)S(1)} %get-tuple-element.32), channel_id=1, source_target_pairs={{0,2},{2,4},{4,6},{6,8},{8,10},{10,12},{12,14},{14,16},{16,18},{18... | collective-permute-start | bytes 98312 | tf_op jit(solution)/shard_map/ppermute | solution.py:33
  37.8 21.3 %collective-permute-start.2 = (bf16[8,2048]{1,0:T(8,128)(2,1)S(1)}, bf16[8,2048]{1,0:T(8,128)(2,1)S(1)}, u32[]{:S(2)}, u32[]{:S(2)}) collective-permute-start(bf16[8,2048]{1,0:T(8,128)(2,1)S(1)} %get-tuple-element.31), channel_id=1, source_target_pairs={{2,0},{4,2},{6,4},{8,6},{10,8},{12,10},{14,12},{16,14},{18,16},{20... | collective-permute-start | bytes 98312 | tf_op jit(solution)/shard_map/ppermute | solution.py:34
  44.7 5.2 %collective-permute-start.6 = (f32[2,8]{1,0:T(2,128)S(1)}, f32[2,8]{1,0:T(2,128)S(1)}, u32[]{:S(2)}, u32[]{:S(2)}) collective-permute-start(f32[2,8]{1,0:T(2,128)S(1)} %get-tuple-element.64), channel_id=1, source_target_pairs={{0,4},{2,6},{4,0},{6,2},{8,12},{10,14},{12,8},{14,10},{16,20},{18,... | collective-permute-start | bytes 200 | tf_op jit(solution)/shard_map/ppermute | solution.py:15
  49.9 4.5 %collective-permute-start.8 = (f32[2,8]{1,0:T(2,128)S(1)}, f32[2,8]{1,0:T(2,128)S(1)}, u32[]{:S(2)}, u32[]{:S(2)}) collective-permute-start(f32[2,8]{1,0:T(2,128)S(1)} %mul.523), channel_id=1, source_target_pairs={{0,8},{2,10},{4,12},{6,14},{8,0},{10,2},{12,4},{14,6},{16,24},{18,... | collective-permute-start | bytes 200 | tf_op jit(solution)/shard_map/ppermute | solution.py:15
  131.0 2.6 copy-start.8
  133.6 0.9 copy-start.4
  133.8 0.7 copy-start.33
  133.9 0.7 copy-start.34
  135.7 74.6 %copy-start.22 = (pred[2]{0:T(512)(128)(4,1)S(1)}, pred[2]{0:T(512)(128)(4,1)}, u32[]{:S(2)}) copy-start(pred[2]{0:T(512)(128)(4,1)} %copy-done.21) | copy-start | bytes 10
  135.7 74.5 %collective-permute-start.3 = (bf16[8,2,64,128]{3,2,1,0:T(8,128)(2,1)S(1)}, bf16[8,2,64,128]{3,2,1,0:T(8,128)(2,1)S(1)}, u32[]{:S(2)}, u32[]{:S(2)}) collective-permute-start(bf16[8,2,64,128]{3,2,1,0:T(8,128)(2,1)S(1)} %fusion.70), channel_id=1, source_target_pairs={{0,2},{2,0},{4,6},{6,4},{8,10},{10,8},{12,14},{14,12},{16,18},{18,... | collective-permute-start | bytes 786440 | tf_op jit(solution)/shard_map/ppermute | solution.py:15
  210.2 2.0 copy-start.26
  210.2 2.0 copy-start.27
  210.2 2.0 copy-start.28
  210.6 8.5 %copy-start.25 = (pred[2]{0:T(512)(128)(4,1)S(1)}, pred[2]{0:T(512)(128)(4,1)}, u32[]{:S(2)}) copy-start(pred[2]{0:T(512)(128)(4,1)} %copy-done.24) | copy-start | bytes 10
  210.6 8.5 %collective-permute-start.5 = (bf16[8,2,64,128]{3,2,1,0:T(8,128)(2,1)S(1)}, bf16[8,2,64,128]{3,2,1,0:T(8,128)(2,1)S(1)}, u32[]{:S(2)}, u32[]{:S(2)}) collective-permute-start(bf16[8,2,64,128]{3,2,1,0:T(8,128)(2,1)S(1)} %fusion.118), channel_id=1, source_target_pairs={{0,4},{2,6},{4,0},{6,2},{8,12},{10,14},{12,8},{14,10},{16,20},{18,... | collective-permute-start | bytes 786440 | tf_op jit(solution)/shard_map/ppermute | solution.py:15
  213.3 7.9 %copy-start.6 = (bf16[48,8,8,128]{3,1,2,0:T(8,128)(2,1)S(1)}, bf16[48,8,8,128]{3,1,2,0:T(8,128)(2,1)}, u32[]{:S(2)}) copy-start(bf16[48,8,8,128]{3,1,2,0:T(8,128)(2,1)} %get-tuple-element.26) | copy-start | bytes 2359300
  220.2 7.9 %collective-permute-start.7 = (bf16[8,2,64,128]{3,2,1,0:T(8,128)(2,1)}, bf16[8,2,64,128]{3,2,1,0:T(8,128)(2,1)}, u32[]{:S(2)}, u32[]{:S(2)}) collective-permute-start(bf16[8,2,64,128]{3,2,1,0:T(8,128)(2,1)} %fusion.90), channel_id=1, source_target_pairs={{0,8},{2,10},{4,12},{6,14},{8,0},{10,2},{12,4},{14,6},{16,24},{18,... | collective-permute-start | bytes 786440 | tf_op jit(solution)/shard_map/ppermute | solution.py:15
  221.2 1.2 copy-start.7
  222.7 1.5 copy-start.10
  222.7 1.5 copy-start.11
  222.7 1.5 copy-start.12
  224.2 4.0 %copy-start.19 = (f32[8,2]{1,0:T(8,128)S(1)}, f32[8,2]{1,0:T(8,128)}, u32[]{:S(2)}) copy-start(f32[8,2]{1,0:T(8,128)} %copy.124) | copy-start | bytes 196
  224.2 4.0 %copy-start.20 = (f32[8,2]{1,0:T(8,128)S(1)}, f32[8,2]{1,0:T(8,128)}, u32[]{:S(2)}) copy-start(f32[8,2]{1,0:T(8,128)} %copy.125) | copy-start | bytes 196
  224.2 4.0 %copy-start.31 = (pred[2]{0:T(512)(128)(4,1)S(1)}, pred[2]{0:T(512)(128)(4,1)}, u32[]{:S(2)}) copy-start(pred[2]{0:T(512)(128)(4,1)} %copy-done.30) | copy-start | bytes 10
  229.6 7.7 %collective-permute-start.9 = (bf16[8,64,128]{2,1,0:T(8,128)(2,1)S(1)}, bf16[8,64,128]{2,1,0:T(8,128)(2,1)S(1)}, u32[]{:S(2)}, u32[]{:S(2)}) collective-permute-start(bf16[8,64,128]{2,1,0:T(8,128)(2,1)S(1)} %fusion.88), channel_id=1, source_target_pairs={{0,16},{2,18},{4,20},{6,22},{8,24},{10,26},{12,28},{14,30},{16,0},... | collective-permute-start | bytes 393224 | tf_op jit(solution)/shard_map/ppermute | solution.py:15
  231.2 6.2 %copy-start.16 = (f32[8,2]{1,0:T(8,128)S(1)}, f32[8,2]{1,0:T(8,128)}, u32[]{:S(2)}) copy-start(f32[8,2]{1,0:T(8,128)} %copy.126) | copy-start | bytes 196
  231.2 6.2 %copy-start.17 = (f32[8,2]{1,0:T(8,128)S(1)}, f32[8,2]{1,0:T(8,128)}, u32[]{:S(2)}) copy-start(f32[8,2]{1,0:T(8,128)} %copy.127) | copy-start | bytes 196
  231.2 6.2 %copy-start.18 = (f32[8,2]{1,0:T(8,128)S(1)}, f32[8,2]{1,0:T(8,128)}, u32[]{:S(2)}) copy-start(f32[8,2]{1,0:T(8,128)} %copy.128) | copy-start | bytes 196
  231.2 6.2 %copy-start.36 = (pred[2]{0:T(512)(128)(4,1)S(1)}, pred[2]{0:T(512)(128)(4,1)}, u32[]{:S(2)}) copy-start(pred[2]{0:T(512)(128)(4,1)} %pad_add_fusion) | copy-start | bytes 10
  238.7 1.1 copy-start.5
  238.7 3.0 %copy-start.9 = (bf16[3,128,8,64]{1,3,0,2:T(8,128)(2,1)S(1)}, bf16[3,128,8,64]{1,3,0,2:T(8,128)(2,1)}, u32[]{:S(2)}) copy-start(bf16[3,128,8,64]{1,3,0,2:T(8,128)(2,1)} %copy.109) | copy-start | bytes 1179652
  239.2 2.5 copy-start.2
  241.7 5.9 %copy-start.15 = (f32[8,64]{1,0:T(8,128)S(1)}, f32[8,64]{1,0:T(8,128)}, u32[]{:S(2)}) copy-start(f32[8,64]{1,0:T(8,128)} %reshape.309) | copy-start | bytes 6148
  247.6 2.3 copy-start.13
  253.1 18.8 %collective-permute-start.10 = (bf16[192,2048]{1,0:T(8,128)(2,1)S(1)}, bf16[192,2048]{1,0:T(8,128)(2,1)S(1)}, u32[]{:S(2)}, u32[]{:S(2)}) collective-permute-start(bf16[192,2048]{1,0:T(8,128)(2,1)S(1)} %fusion.15), channel_id=1, source_target_pairs={{0,1},{1,0},{2,3},{3,2},{4,5},{5,4},{6,7},{7,6},{8,9},{9,8},{10,11... | collective-permute-start | bytes 2359304 | tf_op jit(solution)/shard_map/ppermute | solution.py:15
  271.8 4.1 %copy-start.1 = (bf16[2048,2,8]{0,2,1:T(8,128)(2,1)S(1)}, bf16[2048,2,8]{0,2,1:T(8,128)(2,1)}, u32[]{:S(2)}) copy-start(bf16[2048,2,8]{0,2,1:T(8,128)(2,1)} %param.19) | copy-start | bytes 196612
Sparse Core Ops, SparseCore 0:
  9.8 103.5 all-gather.4
  115.5 88.5 all-gather.2
where the time goes:
time: 283 us
  waiting for transfers between devices  166 us (59%)
  matrix products  30.1 us (11%)
  local copies, waits for them, and re-layouts  29 us (10%)
  other arithmetic  25.2 us (9%)
  starting transfers between devices  18.4 us (7%)
  between operations  14.2 us (5%)
    all_gather x1, waiting for transfers between devices, local(): conv_weight = lax.all_gather(conv_shard, 'sp', axis=0, tiled=True)  68.2 us
    all_gather x1, waiting for transfers between devices, local(): ssd_weight = lax.all_gather(ssd_shard, 'sp', axis=0, tiled=True)  53.7 us
    ppermute x9, waiting for transfers between devices, swapped(): return lax.ppermute(value, axis, [(i, i ^ distance) for i in range(size)])  44 us
    ppermute x9, starting transfers between devices, swapped(): return lax.ppermute(value, axis, [(i, i ^ distance) for i in range(size)])  14.7 us
    unnamed x88, local copies, waits for them, and re-layouts  9.58 us
    dot_general x1, matrix products, local(): jnp.dot(wide_rows, ssd_weight, preferred_element_type=f32).astype(bf16)  8.68 us
    dot_general x2, matrix products, leave(): lax.dot_general(part, exit_weight, (((1,), (1,)), ((), ())), preferred_el...  7.31 us
    dot_general x1, matrix products, local(): jnp.dot(wide_rows, conv_weight[:, :3 * conv_width], preferred_element_typ...  6.02 us
  transfers between devices with their start and end apart: 13, of which 9 were waited for; matrix products, arithmetic and copies ran while one was open for 21% of the time, Pallas kernels for 0%

commit v1 on v0

--- a/solution.py
+++ b/solution.py
@@ -111,7 +111,13 @@
         ],
         axis=1,
     )
-    ssd_weight = lax.all_gather(ssd_shard, "sp", axis=0, tiled=True)
+    devices = lax.axis_size("sp")
+    held, pieces = (ssd_shard, [ssd_shard])
+    for _ in range(devices - 1):
+        held = lax.ppermute(held, "sp", [(i_2, (i_2 + 1) % devices) for i_2 in range(devices)])
+        pieces.insert(0, held)
+    merged = jnp.concatenate(pieces, axis=0)
+    ssd_weight = jnp.roll(merged, (lax.axis_index("sp") + 1) * ssd_shard.shape[0], axis=0)
     float_rows = layer_source_rows.astype(f32)
     normed = (
         float_rows

time: 283 us -> 366 us (1.29)
  waiting for transfers between devices: 166 us -> 239 us
  local copies, waits for them, and re-layouts: 29 us -> 49.8 us
  starting transfers between devices: 18.4 us -> 8.21 us
  matrix products: 30.1 us -> 22.5 us
  other arithmetic: 25.2 us -> 31.1 us
    ppermute x0 -> x15, waiting for transfers between devices: none -> 186 us  [local(): lax.ppermute(held, 'sp', [(i_2, (i_2 + 1) % devices) for i_2 in range(dev...]
    all_gather x1, waiting for transfers between devices: 68.2 us -> 0.02 us  [local(): conv_weight = lax.all_gather(conv_shard, 'sp', axis=0, tiled=True)]
    all_gather x1 -> x0, waiting for transfers between devices: 53.7 us -> none  [local(): ssd_weight = lax.all_gather(ssd_shard, 'sp', axis=0, tiled=True)]
    unnamed x88 -> x140, local copies, waits for them, and re-layouts: 9.58 us -> 34.2 us
    ppermute x9, starting transfers between devices: 14.7 us -> 5.04 us  [swapped(): return lax.ppermute(value, axis, [(i, i ^ distance) for i in range(size)])]
    ppermute x9, waiting for transfers between devices: 44 us -> 53.1 us  [swapped(): return lax.ppermute(value, axis, [(i, i ^ distance) for i in range(size)])]
    dot_general x2, matrix products: 7.31 us -> 2.87 us  [leave(): lax.dot_general(part, exit_weight, (((1,), (1,)), ((), ())), preferred_el...]
  transfers between devices with their start and end apart: 13 -> 27, of which waited for: 9 -> 21; matrix products, arithmetic and copies ran while one was open for 21% -> 23% of each run, Pallas kernels for 0% -> 0%
where the time goes in v1:
time: 366 us; the launch traced here: 365 us
  waiting for transfers between devices  239 us (65%)
  local copies, waits for them, and re-layouts  49.8 us (14%)
  other arithmetic  31.1 us (8%)
  matrix products  22.5 us (6%)
  between operations  14.6 us (4%)
  starting transfers between devices  8.21 us (2%)
    ppermute x15, waiting for transfers between devices, local(): lax.ppermute(held, 'sp', [(i_2, (i_2 + 1) % devices) for i_2 in range(dev...  186 us
    ppermute x9, waiting for transfers between devices, swapped(): return lax.ppermute(value, axis, [(i, i ^ distance) for i in range(size)])  53.1 us
    unnamed x140, local copies, waits for them, and re-layouts  34.2 us
  transfers between devices with their start and end apart: 27, of which 21 were waited for; matrix products, arithmetic and copies ran while one was open for 23% of the time, Pallas kernels for 0%

profile of v1, /device:TPU:0, one launch (start us, length us, event | category | flops | bytes accessed | tf_op | source)
XLA Modules:
  0.0 365.2 jit_solution(15607009707973153050)
XLA Ops:
  9.3 14.7 %collective-permute-done.3 = bf16[128,3072]{1,0:T(8,128)(2,1)S(1)} collective-permute-done((bf16[128,3072]{1,0:T(8,128)(2,1)S(1)}, bf16[128,3072]{1,0:T(8,128)(2,1)S(1)}, u32[]{:S(2)}, u32[]{:S(2)}) %collective-permute-start.3) | collective-permute-done | bytes 786464 | tf_op jit(solution)/shard_map/ppermute | solution.py:117
  23.9 14.1 %collective-permute-done.4 = bf16[128,3072]{1,0:T(8,128)(2,1)S(1)} collective-permute-done((bf16[128,3072]{1,0:T(8,128)(2,1)S(1)}, bf16[128,3072]{1,0:T(8,128)(2,1)S(1)}, u32[]{:S(2)}, u32[]{:S(2)}) %collective-permute-start.4) | collective-permute-done | bytes 786464 | tf_op jit(solution)/shard_map/ppermute | solution.py:117
  39.0 14.1 %collective-permute-done.5 = bf16[128,3072]{1,0:T(8,128)(2,1)S(1)} collective-permute-done((bf16[128,3072]{1,0:T(8,128)(2,1)S(1)}, bf16[128,3072]{1,0:T(8,128)(2,1)S(1)}, u32[]{:S(2)}, u32[]{:S(2)}) %collective-permute-start.5) | collective-permute-done | bytes 786464 | tf_op jit(solution)/shard_map/ppermute | solution.py:117
  54.0 14.1 %collective-permute-done.6 = bf16[128,3072]{1,0:T(8,128)(2,1)S(1)} collective-permute-done((bf16[128,3072]{1,0:T(8,128)(2,1)S(1)}, bf16[128,3072]{1,0:T(8,128)(2,1)S(1)}, u32[]{:S(2)}, u32[]{:S(2)}) %collective-permute-start.6) | collective-permute-done | bytes 786464 | tf_op jit(solution)/shard_map/ppermute | solution.py:117
  69.1 14.1 %collective-permute-done.7 = bf16[128,3072]{1,0:T(8,128)(2,1)S(1)} collective-permute-done((bf16[128,3072]{1,0:T(8,128)(2,1)S(1)}, bf16[128,3072]{1,0:T(8,128)(2,1)S(1)}, u32[]{:S(2)}, u32[]{:S(2)}) %collective-permute-start.7) | collective-permute-done | bytes 786464 | tf_op jit(solution)/shard_map/ppermute | solution.py:117
  84.1 14.1 %collective-permute-done.8 = bf16[128,3072]{1,0:T(8,128)(2,1)S(1)} collective-permute-done((bf16[128,3072]{1,0:T(8,128)(2,1)S(1)}, bf16[128,3072]{1,0:T(8,128)(2,1)S(1)}, u32[]{:S(2)}, u32[]{:S(2)}) %collective-permute-start.8) | collective-permute-done | bytes 786464 | tf_op jit(solution)/shard_map/ppermute | solution.py:117
  99.1 14.2 %collective-permute-done.9 = bf16[128,3072]{1,0:T(8,128)(2,1)} collective-permute-done((bf16[128,3072]{1,0:T(8,128)(2,1)S(1)}, bf16[128,3072]{1,0:T(8,128)(2,1)}, u32[]{:S(2)}, u32[]{:S(2)}) %collective-permute-start.9) | collective-permute-done | bytes 786464 | tf_op jit(solution)/shard_map/ppermute | solution.py:117
  113.3 1.4 fusion.23
  114.9 2.3 constant_dynamic-update-slice_fusion.38
  117.2 1.9 collective-permute-start
  119.1 8.6 %collective-permute-done.10 = bf16[128,3072]{1,0:T(8,128)(2,1)} collective-permute-done((bf16[128,3072]{1,0:T(8,128)(2,1)}, bf16[128,3072]{1,0:T(8,128)(2,1)}, u32[]{:S(2)}, u32[]{:S(2)}) %collective-permute-start.10) | collective-permute-done | bytes 786464 | tf_op jit(solution)/shard_map/ppermute | solution.py:117
  129.6 1.7 copy.147
  134.9 7.2 %collective-permute-done.11 = bf16[128,3072]{1,0:T(8,128)(2,1)} collective-permute-done((bf16[128,3072]{1,0:T(8,128)(2,1)}, bf16[128,3072]{1,0:T(8,128)(2,1)}, u32[]{:S(2)}, u32[]{:S(2)}) %collective-permute-start.11) | collective-permute-done | bytes 786464 | tf_op jit(solution)/shard_map/ppermute | solution.py:117
  143.0 1.8 pad_maximum_fusion.2
  144.8 11.8 %collective-permute-done.12 = bf16[128,3072]{1,0:T(8,128)(2,1)} collective-permute-done((bf16[128,3072]{1,0:T(8,128)(2,1)}, bf16[128,3072]{1,0:T(8,128)(2,1)}, u32[]{:S(2)}, u32[]{:S(2)}) %collective-permute-start.12) | collective-permute-done | bytes 786464 | tf_op jit(solution)/shard_map/ppermute | solution.py:117
  157.9 1.2 constant_dynamic-update-slice_fusion.37
  159.7 11.4 %collective-permute-done.13 = bf16[128,3072]{1,0:T(8,128)(2,1)} collective-permute-done((bf16[128,3072]{1,0:T(8,128)(2,1)}, bf16[128,3072]{1,0:T(8,128)(2,1)}, u32[]{:S(2)}, u32[]{:S(2)}) %collective-permute-start.13) | collective-permute-done | bytes 786464 | tf_op jit(solution)/shard_map/ppermute | solution.py:117
  172.4 1.3 collective-permute-start.1
  173.7 1.3 collective-permute-start.2
  175.0 10.6 %collective-permute-done.14 = bf16[128,3072]{1,0:T(8,128)(2,1)} collective-permute-done((bf16[128,3072]{1,0:T(8,128)(2,1)}, bf16[128,3072]{1,0:T(8,128)(2,1)}, u32[]{:S(2)}, u32[]{:S(2)}) %collective-permute-start.14) | collective-permute-done | bytes 786464 | tf_op jit(solution)/shard_map/ppermute | solution.py:117
  186.3 13.6 %collective-permute-done.15 = bf16[128,3072]{1,0:T(8,128)(2,1)S(1)} collective-permute-done((bf16[128,3072]{1,0:T(8,128)(2,1)}, bf16[128,3072]{1,0:T(8,128)(2,1)S(1)}, u32[]{:S(2)}, u32[]{:S(2)}) %collective-permute-start.15) | collective-permute-done | bytes 786464 | tf_op jit(solution)/shard_map/ppermute | solution.py:117
  202.0 2.2 broadcast_subtract_fusion
  204.1 10.8 %collective-permute-done.16 = bf16[128,3072]{1,0:T(8,128)(2,1)} collective-permute-done((bf16[128,3072]{1,0:T(8,128)(2,1)S(1)}, bf16[128,3072]{1,0:T(8,128)(2,1)}, u32[]{:S(2)}, u32[]{:S(2)}) %collective-permute-start.16) | collective-permute-done | bytes 786464 | tf_op jit(solution)/shard_map/ppermute | solution.py:117
  217.0 12.4 %collective-permute-done.17 = bf16[128,3072]{1,0:T(8,128)(2,1)} collective-permute-done((bf16[128,3072]{1,0:T(8,128)(2,1)}, bf16[128,3072]{1,0:T(8,128)(2,1)}, u32[]{:S(2)}, u32[]{:S(2)}) %collective-permute-start.17) | collective-permute-done | bytes 786464 | tf_op jit(solution)/shard_map/ppermute | solution.py:117
  229.4 1.2 constant_dynamic-update-slice_fusion.34
  230.6 1.2 constant_dynamic-update-slice_fusion.33
  231.9 1.2 constant_dynamic-update-slice_fusion.31
  233.1 1.3 constant_dynamic-update-slice_fusion.30
  234.3 1.3 constant_dynamic-update-slice_fusion.29
  235.6 1.3 constant_dynamic-update-slice_fusion.28
  236.9 1.3 constant_dynamic-update-slice_fusion.27
  238.1 1.3 constant_dynamic-update-slice_fusion.26
  239.9 1.2 constant_dynamic-update-slice_fusion.18
  241.1 1.2 constant_dynamic-update-slice_fusion.17
  242.3 1.2 constant_dynamic-update-slice_fusion.15
  243.5 1.2 constant_dynamic-update-slice_fusion.14
  244.7 1.2 constant_dynamic-update-slice_fusion.13
  245.9 1.2 constant_dynamic-update-slice_fusion.12
  247.1 1.2 constant_dynamic-update-slice_fusion.11
  248.3 1.2 constant_dynamic-update-slice_fusion.10
  249.9 5.6 %fusion.4 = bf16[400,3072]{1,0:T(8,128)(2,1)S(1)} fusion(bf16[400,2048]{1,0:T(8,128)(2,1)S(1)} %constant_dynamic-update-slice_fusion, bf16[4096,3072]{1,0:T(8,128)(2,1)S(1)} %constant_dynamic-update-slice_fusion.3, s32[]{:T(128)S(6)} %select_n.84), kind=kOutput, calls=%fused_computation.4 | convolution fusion | flops 5034393600 | bytes 16678916 | tf_op jit(solution)/shard_map/dot_general | solution.py:164
  255.5 3.2 multiply_convert_fusion
  258.7 1.3 copy-done.2
  260.0 1.3 reshape.312
  261.3 1.6 copy.109
  262.9 2.5 slice_bitcast_fusion.3
  266.6 1.1 fusion.88
  271.6 2.1 collective-permute-start.21
  273.8 12.4 %collective-permute-done.21 = f32[2,8]{1,0:T(2,128)S(1)} collective-permute-done((f32[2,8]{1,0:T(2,128)S(1)}, f32[2,8]{1,0:T(2,128)S(1)}, u32[]{:S(2)}, u32[]{:S(2)}) %collective-permute-start.21) | collective-permute-done | bytes 96 | tf_op jit(solution)/shard_map/ppermute | solution.py:15
  286.3 3.5 collective-permute-done.23
  291.0 2.1 fusion.95
  294.0 1.4 copy.155
  295.3 1.8 reshape.313
  297.1 1.4 copy.135
  298.6 1.4 maximum_bitcast_fusion
  299.9 9.8 %collective-permute-done.22 = bf16[8,2,64,128]{3,2,1,0:T(8,128)(2,1)} collective-permute-done((bf16[8,2,64,128]{3,2,1,0:T(8,128)(2,1)}, bf16[8,2,64,128]{3,2,1,0:T(8,128)(2,1)}, u32[]{:S(2)}, u32[]{:S(2)}) %collective-permute-start.22) | collective-permute-done | bytes 262176 | tf_op jit(solution)/shard_map/ppermute | solution.py:15
  309.7 1.5 fusion.74
  311.5 8.6 %collective-permute-done.24 = bf16[8,64,128]{2,1,0:T(8,128)(2,1)S(1)} collective-permute-done((bf16[8,64,128]{2,1,0:T(8,128)(2,1)S(1)}, bf16[8,64,128]{2,1,0:T(8,128)(2,1)S(1)}, u32[]{:S(2)}, u32[]{:S(2)}) %collective-permute-start.24) | collective-permute-done | bytes 131104 | tf_op jit(solution)/shard_map/ppermute | solution.py:15
  320.2 1.4 add_select_fusion
  322.0 1.9 fusion.54
  323.9 4.1 %multiply_reduce_fusion = (f32[8,3,128]{2,1,0:T(4,128)S(1)}, f32[8,3,128,64]{2,3,1,0:T(8,128)S(1)}) fusion(f32[3,128,8,64]{1,3,0,2:T(8,128)} %copy.135, f32[8,3,128]{2,1,0:T(4,128)S(1)} %copy.133, f32[8,3,128,128]{2,3,1,0:T(8,128)} %fusion.54, f32[8,3,128]{2,1,0:T(4,128)S(1)} %copy.132, bf16[3,128,8,64]{1,3,0,2:T(8,128)(2,1)S(1)} %copy-done.18, ...), kind=kOutput, calls=%fused_computation.75 | convolution fusion | flops 156693504 | bytes 8351744 | tf_op jit(solution)/shard_map/hbts,hbsp->hbtp/dot_general | solution.py:197
  329.2 6.2 %fusion.11 = bf16[400,1536]{1,0:T(8,128)(2,1)S(1)} fusion(bf16[400,2048]{1,0:T(8,128)(2,1)} %copy-done.46, bf16[2048,2560]{0,1:T(8,128)(2,1)} %all-gather.2.cloned.1.call-done), kind=kOutput, calls=%fused_computation.10 | convolution fusion | flops 2517196800 | bytes 9158656 | tf_op jit(solution)/shard_map/dot_general | solution.py:211
  337.8 18.6 %collective-permute-done.25 = bf16[192,2048]{1,0:T(8,128)(2,1)S(1)} collective-permute-done((bf16[192,2048]{1,0:T(8,128)(2,1)S(1)}, bf16[192,2048]{1,0:T(8,128)(2,1)S(1)}, u32[]{:S(2)}, u32[]{:S(2)}) %collective-permute-start.25) | collective-permute-done | bytes 786464 | tf_op jit(solution)/shard_map/ppermute | solution.py:15
  356.4 1.9 add_convert_fusion
  (237 shorter events, 34.0 us)
Async XLA Ops:
  6.5 152.6 %copy-start = (bf16[2048,2,8]{0,2,1:T(8,128)(2,1)S(1)}, bf16[2048,2,8]{0,2,1:T(8,128)(2,1)}, u32[]{:S(2)}) copy-start(bf16[2048,2,8]{0,2,1:T(8,128)(2,1)} %param.19) | copy-start | bytes 196612
  6.5 108.2 %copy-start.38 = (bf16[2048]{0:T(1024)(128)(2,1)S(1)}, bf16[2048]{0:T(1024)(128)(2,1)}, u32[]{:S(2)}) copy-start(bf16[2048]{0:T(1024)(128)(2,1)} %param.15) | copy-start | bytes 12292
  6.5 322.7 %all-gather.2.cloned.1.call-start = ((), (), s32[]{:S(2)}) async-start(), calls=%async_computation | async-start | bytes 11141120 | tf_op jit(solution)/shard_map/all_gather | solution.py:134
  8.6 122.7 %copy-start.23 = (bf16[5,2,1024]{2,1,0:T(2,128)(2,1)S(1)}, bf16[5,2,1024]{2,1,0:T(2,128)(2,1)}, u32[]{:S(2)}) copy-start(bf16[5,2,1024]{2,1,0:T(2,128)(2,1)} %param.22) | copy-start | bytes 61444
  8.7 124.0 %copy-start.35 = (bf16[5,512]{1,0:T(8,128)(2,1)S(1)}, bf16[5,512]{1,0:T(8,128)(2,1)}, u32[]{:S(2)}) copy-start(bf16[5,512]{1,0:T(8,128)(2,1)} %param.21) | copy-start | bytes 15364
  8.7 15.2 %collective-permute-start.3 = (bf16[128,3072]{1,0:T(8,128)(2,1)S(1)}, bf16[128,3072]{1,0:T(8,128)(2,1)S(1)}, u32[]{:S(2)}, u32[]{:S(2)}) collective-permute-start(bf16[128,3072]{1,0:T(8,128)(2,1)S(1)} %pad_maximum_fusion.1), channel_id=1, source_target_pairs={{0,2},{2,4},{4,6},{6,8},{8,10},{10,12},{12,14},{14,16},{16,18},{18... | collective-permute-start | bytes 2359304 | tf_op jit(solution)/shard_map/ppermute | solution.py:117
  23.9 14.1 %collective-permute-start.4 = (bf16[128,3072]{1,0:T(8,128)(2,1)S(1)}, bf16[128,3072]{1,0:T(8,128)(2,1)S(1)}, u32[]{:S(2)}, u32[]{:S(2)}) collective-permute-start(bf16[128,3072]{1,0:T(8,128)(2,1)S(1)} %collective-permute-done.3), channel_id=1, source_target_pairs={{0,2},{2,4},{4,6},{6,8},{8,10},{10,12},{12,14},{14,16},{16,18},{18... | collective-permute-start | bytes 2359304 | tf_op jit(solution)/shard_map/ppermute | solution.py:117
  38.9 14.1 %collective-permute-start.5 = (bf16[128,3072]{1,0:T(8,128)(2,1)S(1)}, bf16[128,3072]{1,0:T(8,128)(2,1)S(1)}, u32[]{:S(2)}, u32[]{:S(2)}) collective-permute-start(bf16[128,3072]{1,0:T(8,128)(2,1)S(1)} %collective-permute-done.4), channel_id=1, source_target_pairs={{0,2},{2,4},{4,6},{6,8},{8,10},{10,12},{12,14},{14,16},{16,18},{18... | collective-permute-start | bytes 2359304 | tf_op jit(solution)/shard_map/ppermute | solution.py:117
  54.0 14.1 %collective-permute-start.6 = (bf16[128,3072]{1,0:T(8,128)(2,1)S(1)}, bf16[128,3072]{1,0:T(8,128)(2,1)S(1)}, u32[]{:S(2)}, u32[]{:S(2)}) collective-permute-start(bf16[128,3072]{1,0:T(8,128)(2,1)S(1)} %collective-permute-done.5), channel_id=1, source_target_pairs={{0,2},{2,4},{4,6},{6,8},{8,10},{10,12},{12,14},{14,16},{16,18},{18... | collective-permute-start | bytes 2359304 | tf_op jit(solution)/shard_map/ppermute | solution.py:117
  69.1 14.1 %collective-permute-start.7 = (bf16[128,3072]{1,0:T(8,128)(2,1)S(1)}, bf16[128,3072]{1,0:T(8,128)(2,1)S(1)}, u32[]{:S(2)}, u32[]{:S(2)}) collective-permute-start(bf16[128,3072]{1,0:T(8,128)(2,1)S(1)} %collective-permute-done.6), channel_id=1, source_target_pairs={{0,2},{2,4},{4,6},{6,8},{8,10},{10,12},{12,14},{14,16},{16,18},{18... | collective-permute-start | bytes 2359304 | tf_op jit(solution)/shard_map/ppermute | solution.py:117
  84.1 14.1 %collective-permute-start.8 = (bf16[128,3072]{1,0:T(8,128)(2,1)S(1)}, bf16[128,3072]{1,0:T(8,128)(2,1)S(1)}, u32[]{:S(2)}, u32[]{:S(2)}) collective-permute-start(bf16[128,3072]{1,0:T(8,128)(2,1)S(1)} %collective-permute-done.7), channel_id=1, source_target_pairs={{0,2},{2,4},{4,6},{6,8},{8,10},{10,12},{12,14},{14,16},{16,18},{18... | collective-permute-start | bytes 2359304 | tf_op jit(solution)/shard_map/ppermute | solution.py:117
  99.1 14.2 %collective-permute-start.9 = (bf16[128,3072]{1,0:T(8,128)(2,1)S(1)}, bf16[128,3072]{1,0:T(8,128)(2,1)}, u32[]{:S(2)}, u32[]{:S(2)}) collective-permute-start(bf16[128,3072]{1,0:T(8,128)(2,1)S(1)} %collective-permute-done.8), channel_id=1, source_target_pairs={{0,2},{2,4},{4,6},{6,8},{8,10},{10,12},{12,14},{14,16},{16,18},{18... | collective-permute-start | bytes 2359304 | tf_op jit(solution)/shard_map/ppermute | solution.py:117
  113.3 14.4 %collective-permute-start.10 = (bf16[128,3072]{1,0:T(8,128)(2,1)}, bf16[128,3072]{1,0:T(8,128)(2,1)}, u32[]{:S(2)}, u32[]{:S(2)}) collective-permute-start(bf16[128,3072]{1,0:T(8,128)(2,1)} %collective-permute-done.9), channel_id=1, source_target_pairs={{0,2},{2,4},{4,6},{6,8},{8,10},{10,12},{12,14},{14,16},{16,18},{18... | collective-permute-start | bytes 2359304 | tf_op jit(solution)/shard_map/ppermute | solution.py:117
  114.7 42.6 %copy-start.45 = (bf16[512]{0:T(512)(128)(2,1)S(1)}, bf16[512]{0:T(512)(128)(2,1)}, u32[]{:S(2)}) copy-start(bf16[512]{0:T(512)(128)(2,1)} %param.25) | copy-start | bytes 3076
  114.7 42.6 %copy-start.27 = (bf16[3,512]{1,0:T(4,128)(2,1)S(1)}, bf16[3,512]{1,0:T(4,128)(2,1)}, u32[]{:S(2)}) copy-start(bf16[3,512]{1,0:T(4,128)(2,1)} %param.20) | copy-start | bytes 9220
  114.7 13.0 %copy-start.19 = (bf16[3,128,512]{2,1,0:T(8,128)(2,1)S(1)}, bf16[3,128,512]{2,1,0:T(8,128)(2,1)}, u32[]{:S(2)}) copy-start(bf16[3,128,512]{2,1,0:T(8,128)(2,1)} %param.16) | copy-start | bytes 1179652
  117.2 53.9 %copy-start.49 = (f32[2,8]{1,0:T(2,128)S(1)}, f32[2,8]{1,0:T(2,128)}, u32[]{:S(2)}) copy-start(f32[2,8]{1,0:T(2,128)} %param.23) | copy-start | bytes 196
  117.2 40.7 %collective-permute-start = (bf16[192,2048]{1,0:T(8,128)(2,1)}, bf16[192,2048]{1,0:T(8,128)(2,1)}, u32[]{:S(2)}, u32[]{:S(2)}) collective-permute-start(bf16[192,2048]{1,0:T(8,128)(2,1)} %get-tuple-element.25), channel_id=1, source_target_pairs={{0,1},{1,0},{2,3},{3,2},{4,5},{5,4},{6,7},{7,6},{8,9},{9,8},{10,11... | collective-permute-start | bytes 2359304 | tf_op jit(solution)/shard_map/ppermute | solution.py:15
  127.7 14.4 %collective-permute-start.11 = (bf16[128,3072]{1,0:T(8,128)(2,1)}, bf16[128,3072]{1,0:T(8,128)(2,1)}, u32[]{:S(2)}, u32[]{:S(2)}) collective-permute-start(bf16[128,3072]{1,0:T(8,128)(2,1)} %collective-permute-done.10), channel_id=1, source_target_pairs={{0,2},{2,4},{4,6},{6,8},{8,10},{10,12},{12,14},{14,16},{16,18},{18... | collective-permute-start | bytes 2359304 | tf_op jit(solution)/shard_map/ppermute | solution.py:117
  142.2 14.4 %collective-permute-start.12 = (bf16[128,3072]{1,0:T(8,128)(2,1)}, bf16[128,3072]{1,0:T(8,128)(2,1)}, u32[]{:S(2)}, u32[]{:S(2)}) collective-permute-start(bf16[128,3072]{1,0:T(8,128)(2,1)} %collective-permute-done.11), channel_id=1, source_target_pairs={{0,2},{2,4},{4,6},{6,8},{8,10},{10,12},{12,14},{14,16},{16,18},{18... | collective-permute-start | bytes 2359304 | tf_op jit(solution)/shard_map/ppermute | solution.py:117
  156.6 14.5 %collective-permute-start.13 = (bf16[128,3072]{1,0:T(8,128)(2,1)}, bf16[128,3072]{1,0:T(8,128)(2,1)}, u32[]{:S(2)}, u32[]{:S(2)}) collective-permute-start(bf16[128,3072]{1,0:T(8,128)(2,1)} %collective-permute-done.12), channel_id=1, source_target_pairs={{0,2},{2,4},{4,6},{6,8},{8,10},{10,12},{12,14},{14,16},{16,18},{18... | collective-permute-start | bytes 2359304 | tf_op jit(solution)/shard_map/ppermute | solution.py:117
  171.1 14.4 %collective-permute-start.14 = (bf16[128,3072]{1,0:T(8,128)(2,1)}, bf16[128,3072]{1,0:T(8,128)(2,1)}, u32[]{:S(2)}, u32[]{:S(2)}) collective-permute-start(bf16[128,3072]{1,0:T(8,128)(2,1)} %collective-permute-done.13), channel_id=1, source_target_pairs={{0,2},{2,4},{4,6},{6,8},{8,10},{10,12},{12,14},{14,16},{16,18},{18... | collective-permute-start | bytes 2359304 | tf_op jit(solution)/shard_map/ppermute | solution.py:117
  172.4 44.5 %collective-permute-start.1 = (bf16[8,2048]{1,0:T(8,128)(2,1)S(1)}, bf16[8,2048]{1,0:T(8,128)(2,1)S(1)}, u32[]{:S(2)}, u32[]{:S(2)}) collective-permute-start(bf16[8,2048]{1,0:T(8,128)(2,1)S(1)} %get-tuple-element.32), channel_id=1, source_target_pairs={{0,2},{2,4},{4,6},{6,8},{8,10},{10,12},{12,14},{14,16},{16,18},{18... | collective-permute-start | bytes 98312 | tf_op jit(solution)/shard_map/ppermute | solution.py:33
  173.7 43.3 %collective-permute-start.2 = (bf16[8,2048]{1,0:T(8,128)(2,1)S(1)}, bf16[8,2048]{1,0:T(8,128)(2,1)S(1)}, u32[]{:S(2)}, u32[]{:S(2)}) collective-permute-start(bf16[8,2048]{1,0:T(8,128)(2,1)S(1)} %get-tuple-element.31), channel_id=1, source_target_pairs={{2,0},{4,2},{6,4},{8,6},{10,8},{12,10},{14,12},{16,14},{18,16},{20... | collective-permute-start | bytes 98312 | tf_op jit(solution)/shard_map/ppermute | solution.py:34
  185.5 14.3 %collective-permute-start.15 = (bf16[128,3072]{1,0:T(8,128)(2,1)}, bf16[128,3072]{1,0:T(8,128)(2,1)S(1)}, u32[]{:S(2)}, u32[]{:S(2)}) collective-permute-start(bf16[128,3072]{1,0:T(8,128)(2,1)} %collective-permute-done.14), channel_id=1, source_target_pairs={{0,2},{2,4},{4,6},{6,8},{8,10},{10,12},{12,14},{14,16},{16,18},{18... | collective-permute-start | bytes 2359304 | tf_op jit(solution)/shard_map/ppermute | solution.py:117
  185.6 45.0 %copy-start.28 = (f32[2,8]{1,0:T(2,128)}, f32[2,8]{1,0:T(2,128)S(1)}, u32[]{:S(2)}) copy-start(f32[2,8]{1,0:T(2,128)S(1)} %get-tuple-element.55) | copy-start | bytes 196
  200.7 14.2 %collective-permute-start.16 = (bf16[128,3072]{1,0:T(8,128)(2,1)S(1)}, bf16[128,3072]{1,0:T(8,128)(2,1)}, u32[]{:S(2)}, u32[]{:S(2)}) collective-permute-start(bf16[128,3072]{1,0:T(8,128)(2,1)S(1)} %collective-permute-done.15), channel_id=1, source_target_pairs={{0,2},{2,4},{4,6},{6,8},{8,10},{10,12},{12,14},{14,16},{16,18},{18... | collective-permute-start | bytes 2359304 | tf_op jit(solution)/shard_map/ppermute | solution.py:117
  215.0 14.4 %collective-permute-start.17 = (bf16[128,3072]{1,0:T(8,128)(2,1)}, bf16[128,3072]{1,0:T(8,128)(2,1)}, u32[]{:S(2)}, u32[]{:S(2)}) collective-permute-start(bf16[128,3072]{1,0:T(8,128)(2,1)} %collective-permute-done.16), channel_id=1, source_target_pairs={{0,2},{2,4},{4,6},{6,8},{8,10},{10,12},{12,14},{14,16},{16,18},{18... | collective-permute-start | bytes 2359304 | tf_op jit(solution)/shard_map/ppermute | solution.py:117
  216.2 52.3 %collective-permute-start.19 = (f32[2,8]{1,0:T(2,128)}, f32[2,8]{1,0:T(2,128)}, u32[]{:S(2)}, u32[]{:S(2)}) collective-permute-start(f32[2,8]{1,0:T(2,128)} %exp.52), channel_id=1, source_target_pairs={{0,2},{2,0},{4,6},{6,4},{8,10},{10,8},{12,14},{14,12},{16,18},{18,... | collective-permute-start | bytes 200 | tf_op jit(solution)/shard_map/ppermute | solution.py:15
  216.9 14.9 %copy-start.14 = (bf16[128,3072]{1,0:T(8,128)(2,1)S(1)}, bf16[128,3072]{1,0:T(8,128)(2,1)}, u32[]{:S(2)}) copy-start(bf16[128,3072]{1,0:T(8,128)(2,1)} %copy-done.13) | copy-start | bytes 2359300
  217.0 32.9 %copy-start.46 = (bf16[400,2048]{1,0:T(8,128)(2,1)}, bf16[400,2048]{1,0:T(8,128)(2,1)S(1)}, u32[]{:S(2)}) copy-start(bf16[400,2048]{1,0:T(8,128)(2,1)S(1)} %constant_dynamic-update-slice_fusion) | copy-start | bytes 4915204
  233.0 6.4 %copy-start.12 = (bf16[128,3072]{1,0:T(8,128)(2,1)S(1)}, bf16[128,3072]{1,0:T(8,128)(2,1)}, u32[]{:S(2)}) copy-start(bf16[128,3072]{1,0:T(8,128)(2,1)} %copy-done.11) | copy-start | bytes 2359300
  234.3 5.2 %copy-start.10 = (bf16[128,3072]{1,0:T(8,128)(2,1)S(1)}, bf16[128,3072]{1,0:T(8,128)(2,1)}, u32[]{:S(2)}) copy-start(bf16[128,3072]{1,0:T(8,128)(2,1)} %copy-done.9) | copy-start | bytes 2359300
  235.6 4.0 %copy-start.8 = (bf16[128,3072]{1,0:T(8,128)(2,1)S(1)}, bf16[128,3072]{1,0:T(8,128)(2,1)}, u32[]{:S(2)}) copy-start(bf16[128,3072]{1,0:T(8,128)(2,1)} %copy-done.7) | copy-start | bytes 2359300
  262.9 3.7 %copy-start.39 = (f32[8]{0:T(128)S(1)}, f32[8]{0:T(128)}, u32[]{:S(2)}) copy-start(f32[8]{0:T(128)} %get-tuple-element.57) | copy-start | bytes 100
  262.9 3.7 %copy-start.40 = (f32[8]{0:T(128)S(1)}, f32[8]{0:T(128)}, u32[]{:S(2)}) copy-start(f32[8]{0:T(128)} %get-tuple-element.58) | copy-start | bytes 100
  262.9 3.7 %copy-start.41 = (f32[8]{0:T(128)S(1)}, f32[8]{0:T(128)}, u32[]{:S(2)}) copy-start(f32[8]{0:T(128)} %get-tuple-element.59) | copy-start | bytes 100
  262.9 3.6 copy-start.42
  262.9 3.6 copy-start.43
  262.9 3.6 copy-start.44
  265.7 4.5 %copy-start.26 = (pred[2]{0:T(512)(128)(4,1)S(1)}, pred[2]{0:T(512)(128)(4,1)}, u32[]{:S(2)}) copy-start(pred[2]{0:T(512)(128)(4,1)} %pad_add_fusion.3) | copy-start | bytes 10
  265.9 5.3 %copy-start.36 = (f32[1,8,3]{1,0,2:T(1,128)S(1)}, f32[1,8,3]{1,0,2:T(1,128)}, u32[]{:S(2)}) copy-start(f32[1,8,3]{1,0,2:T(1,128)} %reduce-window_subtract_fusion) | copy-start | bytes 292
  265.9 5.6 %copy-start.22 = (f32[8,3,128]{2,0,1:T(8,128)S(1)}, f32[8,3,128]{2,0,1:T(8,128)}, u32[]{:S(2)}) copy-start(f32[8,3,128]{2,0,1:T(8,128)} %get-tuple-element.44) | copy-start | bytes 36868
  265.9 5.6 %copy-start.20 = (f32[8,3,128]{2,0,1:T(8,128)S(1)}, f32[8,3,128]{2,0,1:T(8,128)}, u32[]{:S(2)}) copy-start(f32[8,3,128]{2,0,1:T(8,128)} %get-tuple-element.45) | copy-start | bytes 36868
  265.9 5.7 %copy-start.21 = (f32[8,3,128]{2,0,1:T(8,128)S(1)}, f32[8,3,128]{2,0,1:T(8,128)}, u32[]{:S(2)}) copy-start(f32[8,3,128]{2,0,1:T(8,128)} %get-tuple-element.48) | copy-start | bytes 36868
  265.9 24.0 %copy-start.30 = (pred[2]{0:T(512)(128)(4,1)S(1)}, pred[2]{0:T(512)(128)(4,1)}, u32[]{:S(2)}) copy-start(pred[2]{0:T(512)(128)(4,1)} %pad_add_fusion.2) | copy-start | bytes 10
  268.5 1.7 collective-permute-start.18
  271.2 19.7 %collective-permute-start.20 = (bf16[8,2,64,128]{3,2,1,0:T(8,128)(2,1)}, bf16[8,2,64,128]{3,2,1,0:T(8,128)(2,1)}, u32[]{:S(2)}, u32[]{:S(2)}) collective-permute-start(bf16[8,2,64,128]{3,2,1,0:T(8,128)(2,1)} %fusion.124), channel_id=1, source_target_pairs={{0,4},{2,6},{4,0},{6,2},{8,12},{10,14},{12,8},{14,10},{16,20},{18,... | collective-permute-start | bytes 786440 | tf_op jit(solution)/shard_map/ppermute | solution.py:15
  271.6 14.6 %collective-permute-start.21 = (f32[2,8]{1,0:T(2,128)S(1)}, f32[2,8]{1,0:T(2,128)S(1)}, u32[]{:S(2)}, u32[]{:S(2)}) collective-permute-start(f32[2,8]{1,0:T(2,128)S(1)} %get-tuple-element.64), channel_id=1, source_target_pairs={{0,4},{2,6},{4,0},{6,2},{8,12},{10,14},{12,8},{14,10},{16,20},{18,... | collective-permute-start | bytes 200 | tf_op jit(solution)/shard_map/ppermute | solution.py:15
  286.3 3.6 collective-permute-start.23
  293.0 16.7 %collective-permute-start.22 = (bf16[8,2,64,128]{3,2,1,0:T(8,128)(2,1)}, bf16[8,2,64,128]{3,2,1,0:T(8,128)(2,1)}, u32[]{:S(2)}, u32[]{:S(2)}) collective-permute-start(bf16[8,2,64,128]{3,2,1,0:T(8,128)(2,1)} %fusion.95), channel_id=1, source_target_pairs={{0,8},{2,10},{4,12},{6,14},{8,0},{10,2},{12,4},{14,6},{16,24},{18,... | collective-permute-start | bytes 786440 | tf_op jit(solution)/shard_map/ppermute | solution.py:15
  295.3 14.4 %copy-start.37 = (pred[2]{0:T(512)(128)(4,1)S(1)}, pred[2]{0:T(512)(128)(4,1)}, u32[]{:S(2)}) copy-start(pred[2]{0:T(512)(128)(4,1)} %pad_add_fusion.1) | copy-start | bytes 10
  298.5 21.6 %copy-start.47 = (pred[2]{0:T(512)(128)(4,1)S(1)}, pred[2]{0:T(512)(128)(4,1)}, u32[]{:S(2)}) copy-start(pred[2]{0:T(512)(128)(4,1)} %pad_add_fusion) | copy-start | bytes 10
  311.2 8.9 %collective-permute-start.24 = (bf16[8,64,128]{2,1,0:T(8,128)(2,1)S(1)}, bf16[8,64,128]{2,1,0:T(8,128)(2,1)S(1)}, u32[]{:S(2)}, u32[]{:S(2)}) collective-permute-start(bf16[8,64,128]{2,1,0:T(8,128)(2,1)S(1)} %fusion.93), channel_id=1, source_target_pairs={{0,16},{2,18},{4,20},{6,22},{8,24},{10,26},{12,28},{14,30},{16,0},... | collective-permute-start | bytes 393224 | tf_op jit(solution)/shard_map/ppermute | solution.py:15
  311.5 12.4 %copy-start.16 = (bf16[48,8,8,128]{3,2,1,0:T(8,128)(2,1)S(1)}, bf16[48,8,8,128]{3,2,1,0:T(8,128)(2,1)}, u32[]{:S(2)}) copy-start(bf16[48,8,8,128]{3,2,1,0:T(8,128)(2,1)} %copy-done.15) | copy-start | bytes 2359300
  311.5 12.4 %copy-start.18 = (bf16[3,128,8,64]{1,3,0,2:T(8,128)(2,1)S(1)}, bf16[3,128,8,64]{1,3,0,2:T(8,128)(2,1)}, u32[]{:S(2)}) copy-start(bf16[3,128,8,64]{1,3,0,2:T(8,128)(2,1)} %copy-done.17) | copy-start | bytes 1179652
  311.5 12.4 %copy-start.24 = (pred[128,128]{1,0:T(8,128)(4,1)S(1)}, pred[128,128]{1,0:T(8,128)(4,1)}, u32[]{:S(2)}) copy-start(pred[128,128]{1,0:T(8,128)(4,1)} %get-tuple-element.70) | copy-start | bytes 49156
  311.5 12.4 %copy-start.25 = (pred[128,128]{1,0:T(8,128)(4,1)S(1)}, pred[128,128]{1,0:T(8,128)(4,1)}, u32[]{:S(2)}) copy-start(pred[128,128]{1,0:T(8,128)(4,1)} %get-tuple-element.71) | copy-start | bytes 49156
  329.2 6.3 %copy-start.31 = (f32[1,512]{1,0:T(1,128)S(1)}, f32[1,512]{1,0:T(1,128)}, u32[]{:S(2)}) copy-start(f32[1,512]{1,0:T(1,128)} %get-tuple-element.52) | copy-start | bytes 6148
  329.2 6.3 %copy-start.32 = (f32[1,512]{1,0:T(1,128)S(1)}, f32[1,512]{1,0:T(1,128)}, u32[]{:S(2)}) copy-start(f32[1,512]{1,0:T(1,128)} %get-tuple-element.53) | copy-start | bytes 6148
  329.2 6.3 %copy-start.33 = (f32[1,512]{1,0:T(1,128)S(1)}, f32[1,512]{1,0:T(1,128)}, u32[]{:S(2)}) copy-start(f32[1,512]{1,0:T(1,128)} %get-tuple-element.54) | copy-start | bytes 6148
  329.2 6.7 %copy-start.48 = (bf16[2048,2560]{0,1:T(8,128)(2,1)S(1)}, bf16[2048,2560]{0,1:T(8,128)(2,1)}, u32[]{:S(2)}) copy-start(bf16[2048,2560]{0,1:T(8,128)(2,1)} %all-gather.2.cloned.1.call-done) | copy-start | bytes 31457284
  335.9 22.4 %copy-start.1 = (bf16[2048,2,8]{0,2,1:T(8,128)(2,1)S(1)}, bf16[2048,2,8]{0,2,1:T(8,128)(2,1)}, u32[]{:S(2)}) copy-start(bf16[2048,2,8]{0,2,1:T(8,128)(2,1)} %param.19) | copy-start | bytes 196612
  336.9 19.6 %collective-permute-start.25 = (bf16[192,2048]{1,0:T(8,128)(2,1)S(1)}, bf16[192,2048]{1,0:T(8,128)(2,1)S(1)}, u32[]{:S(2)}, u32[]{:S(2)}) collective-permute-start(bf16[192,2048]{1,0:T(8,128)(2,1)S(1)} %fusion.20), channel_id=1, source_target_pairs={{0,1},{1,0},{2,3},{3,2},{4,5},{5,4},{6,7},{7,6},{8,9},{9,8},{10,11... | collective-permute-start | bytes 2359304 | tf_op jit(solution)/shard_map/ppermute | solution.py:15
  (13 other events, 21.1 us)
Sparse Core Ops, SparseCore 0:
  217.0 97.4 all-gather.1
